TPU v7x, 32 devices: a whole 2x2x4 slice. The times are simulated.
32 devices in a mesh: sp: 16 (over z, y, x), tp: 2 (over core).
Axes of the slice: x: 2, y: 2, z: 4, core: 2. Of those that a mesh axis runs over, the one named last changes fastest.
Arguments:
- resid: bfloat16 [8192, 2048], P('sp'), may hold values from -6 to 6
- queries: bfloat16 [8192, 2048], P('sp', 'tp'), may hold values from -6 to 6
- keys: bfloat16 [8192, 512], P('sp', 'tp'), may hold values from -6 to 6
- values: bfloat16 [8192, 512], P('sp', 'tp'), may hold values from -6 to 6
- documents: int32 [8192], P('sp'), may hold values from 0 to 7, never falling along the last dimension, each value on 1 to 2048 neighbouring positions
- q_gain: float32 [64], replicated, may hold values from 0.5 to 6.5
- k_gain: float32 [64], replicated, may hold values from 0.5 to 6.5
- sink: float32 [32], P('tp'), may hold values from -1 to 5
- w_out: bfloat16 [2048, 2048], P('tp'), may hold values from -0.5 to 0.5
- n_gain: float32 [2048], replicated, may hold values from 0.1 to 1.9
- w_up: bfloat16 [2048, 8192], P('sp', 'tp'), may hold values from -0.125 to 0.125
- w_down: bfloat16 [8192, 2048], P('tp', 'sp'), may hold values from -0.0625 to 0.0625
Outputs:
- layer_out: bfloat16 [8192, 2048], P('sp')
All inputs are finite; a program needn't handle non-finite values.
Results may differ from a plain program's by a relative error of at most 0.018.
The roundings to bfloat16 on the way count: a program that leaves them out, or rounds other values in their place, can miss the bound.
Values may be sent and summed in bfloat16 or wider, within the bound.
A program may use at most 128 MiB of HBM per device.

v0:
```python
import functools

import jax
import jax.numpy as jnp
from jax import lax
from jax.experimental import pallas as pl
from jax.experimental.pallas import tpu as pltpu
from jax.sharding import PartitionSpec as P

WINDOW = 128
EPS = 1e-06
MEMBERS = 4
F32 = jnp.float32
BF16 = jnp.bfloat16
MESH = pl.DeviceIdType.MESH


def rms(wide, gain):
    return wide * lax.rsqrt(jnp.mean(wide * wide, axis=-1, keepdims=True) + EPS) * gain


def kernel(
    n_sp,
    head,
    heads,
    kv_heads,
    resid,
    queries,
    keys,
    values,
    doc_col,
    doc_row,
    q_gain,
    k_gain,
    slopes,
    sink,
    w_out,
    n_gain,
    w_up,
    w_down,
    out,
    kx,
    vx,
    dx,
    kn,
    att,
    wo,
    res,
    mine,
    other,
    other_in,
    mid,
    normed,
    wu,
    wd,
    act,
    part,
    twin_out,
    twin_in,
    sum_out,
    sum_in,
    half_out,
    half_in,
    halo_send,
    halo_recv,
    w_send,
    w_recv,
    w_local,
    loc_sem,
    tok_send,
    tok_recv,
    pair_send,
    pair_recv,
    swap_send,
    swap_recv,
    misc_send,
    misc_recv,
):
    rows = queries.shape[0]
    half = rows // 2
    depth = w_up.shape[0]
    units = wu.shape[1]
    width = wd.shape[1]
    group = heads // kv_heads
    n_za = n_sp // 8

    sp = lax.axis_index("sp")
    t = lax.axis_index("tp")
    u = 1 - t
    x = sp % 2
    y = (sp // 2) % 2
    zb = (sp // 4) % 2
    za = sp // 8
    me = zb * 2 + x

    def index(za_, zb_, y_, x_):
        return za_ * 8 + zb_ * 4 + y_ * 2 + x_

    def flip(v, by):
        return 1 - v if by else v

    def remote(src, dst, send, recv, where):
        return pltpu.make_async_remote_copy(
            src_ref=src, dst_ref=dst, send_sem=send, recv_sem=recv,
            device_id=where, device_id_type=MESH,
        )

    up_to = lax.rem(sp + 1, n_sp)
    down_to = lax.rem(sp + n_sp - 1, n_sp)
    partners = [(sp, u), (up_to, t), (down_to, t), (index(za, zb, 1 - y, x), t)]
    partners += [(index(za, flip(zb, fz), y, flip(x, fx)), t) for fz, fx in ((0, 1), (1, 0), (1, 1))]
    partners += [(index(lax.rem(za + d, n_za), zb, y, x), t) for d in range(1, n_za)]
    with jax.named_scope("barrier"):
        greeting = pltpu.get_barrier_semaphore()
        for where in partners:
            pl.semaphore_signal(greeting, inc=1, device_id=where, device_id_type=MESH)
        pl.semaphore_wait(greeting, len(partners))

    load_wo = pltpu.make_async_copy(w_out, wo, loc_sem.at[0])
    load_wo.start()
    load_res = pltpu.make_async_copy(resid.at[pl.ds(t * half, half), :], res, loc_sem.at[1])
    load_res.start()
    own_k = pltpu.make_async_copy(keys, kx.at[pl.ds(WINDOW, rows), :], loc_sem.at[2])
    own_v = pltpu.make_async_copy(values, vx.at[pl.ds(WINDOW, rows), :], loc_sem.at[3])
    own_d = pltpu.make_async_copy(doc_row, dx.at[:, pl.ds(WINDOW, rows)], loc_sem.at[4])
    own_k.start()
    own_v.start()
    own_d.start()

    def halo(side, where):
        src = rows - WINDOW if side == 0 else 0
        dst = 0 if side == 0 else WINDOW + rows
        return [
            remote(keys.at[pl.ds(src, WINDOW), :], kx.at[pl.ds(dst, WINDOW), :],
                   halo_send.at[side, 0], halo_recv.at[side, 0], where),
            remote(values.at[pl.ds(src, WINDOW), :], vx.at[pl.ds(dst, WINDOW), :],
                   halo_send.at[side, 1], halo_recv.at[side, 1], where),
            remote(doc_row.at[:, pl.ds(src, WINDOW)], dx.at[:, pl.ds(dst, WINDOW)],
                   halo_send.at[side, 2], halo_recv.at[side, 2], where),
        ]

    @pl.when(sp < n_sp - 1)
    def _():
        for c in halo(0, (up_to, t)):
            c.start()

    @pl.when(sp > 0)
    def _():
        for c in halo(1, (down_to, t)):
            c.start()

    def place(w, s):
        if w == 0:
            return wu.at[pl.ds(pl.multiple_of(s * depth, depth), depth), :]
        return wd.at[:, pl.ds(pl.multiple_of(s * depth, depth), depth)]

    def source(w, m):
        at = pl.ds(pl.multiple_of(m * units, units), units)
        return w_up.at[:, at] if w == 0 else w_down.at[at, :]

    flips = ((0, 1), (1, 0), (1, 1))

    def first_copy(w, k):
        fz, fx = flips[k]
        zb_, x_ = flip(zb, fz), flip(x, fx)
        return remote(source(w, zb_ * 2 + x_), place(w, sp), w_send.at[w, k], w_recv.at[w, sp],
                      (index(za, zb_, y, x_), t))

    locals_ = [pltpu.make_async_copy(source(w, me), place(w, sp), w_local.at[w]) for w in range(2)]
    def arrived(w, s):
        remote(place(w, s), place(w, s), w_send.at[w, 0], w_recv.at[w, s], (sp, u)).wait_recv()

    sent = [[], []]

    def start(w, s, where, src=None):
        c = remote(place(w, s) if src is None else src, place(w, s), w_send.at[w, 3 + len(sent[w])],
                   w_recv.at[w, s], where)
        c.start()
        sent[w].append(c)

    def onward(w, s, src=None):
        for d in range(1, n_za):
            start(w, s, (index(lax.rem(za + d, n_za), zb, y, x), t), src)
        start(w, s, (index(za, zb, 1 - y, x), t), src)

    def exchange(w):
        for k in range(3):
            first_copy(w, k).start()
        locals_[w].start()

    def spread_own(w):
        onward(w, sp, source(w, me))

    def spread(w):
        with jax.named_scope(f"spread#w={w}"):
            for fz, fx in flips:
                s = index(za, flip(zb, fz), y, flip(x, fx))
                arrived(w, s)
                onward(w, s)

    def relay(w, k):
        fz, fx = ((0, 0),) [0] if k == 0 else flips[k - 1]
        with jax.named_scope(f"relay#w={w}#k={k}"):
            for d in range(1, n_za):
                s = index(lax.rem(za + n_za - d, n_za), flip(zb, fz), y, flip(x, fx))
                arrived(w, s)
                start(w, s, (index(za, zb, 1 - y, x), t))

    def finish(w):
        with jax.named_scope(f"finish#w={w}"):
            locals_[w].wait()
            for a in range(n_za):
                for k in range(4):
                    arrived(w, index(a, k // 2, 1 - y, k % 2))

    exchange(0)
    spread_own(0)

    with jax.named_scope("own_wait"):
        own_k.wait()
        own_v.wait()
        own_d.wait()

    @pl.when(sp > 0)
    def _():
        for c in halo(0, (down_to, t)):
            c.wait_recv()

    @pl.when(sp == 0)
    def _():
        kx[pl.ds(0, WINDOW), :] = jnp.zeros((WINDOW, kx.shape[1]), BF16)
        vx[pl.ds(0, WINDOW), :] = jnp.zeros((WINDOW, vx.shape[1]), BF16)
        dx[:, pl.ds(0, WINDOW)] = jnp.full((8, WINDOW), -1, jnp.int32)

    @pl.when(sp < n_sp - 1)
    def _():
        for c in halo(1, (up_to, t)):
            c.wait_recv()

    @pl.when(sp == n_sp - 1)
    def _():
        end = WINDOW + rows
        kx[pl.ds(end, WINDOW), :] = jnp.zeros((WINDOW, kx.shape[1]), BF16)
        vx[pl.ds(end, WINDOW), :] = jnp.zeros((WINDOW, vx.shape[1]), BF16)
        dx[:, pl.ds(end, WINDOW)] = jnp.full((8, WINDOW), -1, jnp.int32)

    def norm_keys(b, carry):
        at = pl.ds(pl.multiple_of(b * WINDOW, WINDOW), WINDOW)
        block = kx[at, :].astype(F32)
        kn[at, :] = jnp.concatenate(
            [rms(block[:, k * head:(k + 1) * head], k_gain[...]) for k in range(kv_heads)], axis=1
        ).astype(BF16)
        return carry

    exchange(1)
    with jax.named_scope("norm_keys"):
        lax.fori_loop(0, kx.shape[0] // WINDOW, norm_keys, 0)

    span = 3 * WINDOW

    def attend(b, carry):
        at = pl.ds(pl.multiple_of(b * WINDOW, WINDOW), WINDOW)
        near = pl.ds(pl.multiple_of(b * WINDOW, WINDOW), span)
        far = jnp.abs(
            lax.broadcasted_iota(jnp.int32, (WINDOW, span), 1)
            - lax.broadcasted_iota(jnp.int32, (WINDOW, span), 0) - WINDOW
        )
        allowed = (far <= WINDOW) & (dx[0:1, near] == doc_col[at, :])
        mask = jnp.where(allowed, F32(0.0), F32(-1e30))
        far = far.astype(F32)
        for k in range(kv_heads):
            lanes = slice(k * head, (k + 1) * head)
            kb = kn[near, lanes]
            vb = vx[near, lanes]
            done = []
            for g in range(group):
                h = k * group + g
                qb = rms(queries[at, h * head:(h + 1) * head].astype(F32), q_gain[...]).astype(BF16)
                score = lax.dot_general(
                    qb, kb, (((1,), (1,)), ((), ())), preferred_element_type=F32
                ) * (head ** -0.5)
                score = (score - slopes[h] * far) + mask
                top = jnp.maximum(jnp.max(score, axis=-1, keepdims=True), sink[h])
                p = jnp.exp(score - top)
                denom = jnp.sum(p, axis=-1, keepdims=True) + jnp.exp(sink[h] - top)
                summed = jnp.dot(p.astype(BF16), vb, preferred_element_type=F32)
                done.append((summed / denom).astype(BF16))
                if len(done) == 2:
                    att[at, (h - 1) * head:(h + 1) * head] = jnp.concatenate(done, axis=1)
                    done = []
        return carry

    tile = 256
    rounds = half // WINDOW
    swaps = []

    def project(row, dest):
        lhs = att[pl.ds(pl.multiple_of(row, WINDOW), WINDOW), :]

        def step(j, carry):
            cols = pl.ds(pl.multiple_of(j * tile, tile), tile)
            dest[:, cols] = jnp.dot(lhs, wo[:, cols], preferred_element_type=F32).astype(BF16)
            return carry

        lax.fori_loop(0, width // tile, step, 0)

    def token_rows(slot, r):
        return normed.at[pl.ds(pl.multiple_of(slot * half + r * WINDOW, WINDOW), WINDOW), :]

    def token_copy(k, r):
        fz, fx = flips[k]
        where = (index(za, flip(zb, fz), y, flip(x, fx)), t)
        rows_ = token_rows(me * 2 + t, r)
        return remote(rows_, rows_, tok_send.at[k, r], tok_recv.at[k, r], where)

    def member(k):
        if k == 3:
            return me
        fz, fx = flips[k]
        return flip(zb, fz) * 2 + flip(x, fx)

    def pair_copy(k, core, r):
        rows_ = token_rows(member(k) * 2 + core, r)
        return remote(rows_, rows_, pair_send.at[k, r], pair_recv.at[k, r], (sp, u))

    def token_pass(k, r):
        with jax.named_scope(f"token#k={k}#r={r}"):
            rows_ = token_rows(member(k) * 2 + t, r)
            remote(rows_, rows_, tok_send.at[k, r], tok_recv.at[k, r], (sp, u)).wait_recv()
            if k == 1:
                token_relay(r).start()
            pair_copy(k, t, r).start()

    def token_relay(r):
        rows_ = token_rows(member(1) * 2 + t, r)
        return remote(rows_, rows_, tok_send.at[2, r], tok_recv.at[2, r],
                      (index(za, zb, y, 1 - x), t))

    def one_round(r):
        with jax.named_scope("project"):
            project(u * half + r * WINDOW, other.at[r])
            swap = remote(other.at[r], other_in.at[r], swap_send.at[r], swap_recv.at[r], (sp, u))
            swap.start()
            swaps.append(swap)
            project(t * half + r * WINDOW, mine.at[r])
        with jax.named_scope("swap_wait"):
            swap.wait_recv()

        def middle(i, carry):
            at = pl.ds(pl.multiple_of(i * 64, 64), 64)
            here = pl.ds(pl.multiple_of(r * WINDOW + i * 64, 64), 64)
            both = mine[r, at, :].astype(F32) + other_in[r, at, :].astype(F32)
            value = (res[here, :].astype(F32) + both).astype(BF16)
            mid[here, :] = value
            row = pl.multiple_of((me * 2 + t) * half + r * WINDOW + i * 64, 64)
            normed[pl.ds(row, 64), :] = rms(value.astype(F32), n_gain[...]).astype(BF16)
            return carry

        lax.fori_loop(0, WINDOW // 64, middle, 0)
        for k in (1, 0):
            token_copy(k, r).start()
        pair_copy(3, t, r).start()

    def attend_pair(r, between):
        with jax.named_scope("attend"):
            lax.fori_loop(r, r + 1, attend, 0)
        between()
        with jax.named_scope("attend"):
            lax.fori_loop(r + rounds, r + rounds + 1, attend, 0)

    for r in range(rounds):
        if r == 0:
            attend_pair(r, lambda: spread(0))
            spread_own(1)
            load_wo.wait()
            load_res.wait()
        elif r == 1:
            attend_pair(r, lambda: relay(0, 0))
            relay(0, 1)
        else:
            attend_pair(r, lambda: None)
        one_round(r)

    def up(m):
        row = pl.multiple_of(m * rows, rows)

        def step(j, carry):
            cols = pl.ds(pl.multiple_of(j * tile, tile), tile)
            v = jnp.dot(normed[pl.ds(row, rows), :], wu[:, cols], preferred_element_type=F32)
            v = jnp.maximum(v, 0.0)
            act[pl.ds(row, rows), cols] = (v * v).astype(BF16)
            return carry

        with jax.named_scope("up"):
            lax.fori_loop(0, units // tile, step, 0)

    def pair_wait(k):
        with jax.named_scope("pair_wait"):
            for r in range(rounds):
                pair_copy(k, u, r).wait_recv()

    spread(1)
    if rounds < 2:
        relay(0, 0)
        relay(0, 1)
    for r in range(rounds - 1):
        token_pass(1, r)
    relay(0, 2)
    relay(0, 3)
    token_pass(1, rounds - 1)
    relay(1, 0)
    finish(0)
    pair_wait(3)
    up(me)
    for r in range(rounds):
        token_pass(0, r)
    relay(1, 1)
    pair_wait(0)
    up(member(0))
    for r in range(rounds):
        token_pass(2, r)
    relay(1, 2)
    relay(1, 3)
    for k in (1, 2):
        pair_wait(k)
        up(member(k))
    finish(1)

    def twin_copy(i):
        return remote(twin_out.at[i], twin_in.at[i], misc_send.at[1 + i], misc_recv.at[1 + i], (sp, u))

    def sum_copy(i, where):
        return remote(sum_out.at[i], sum_in.at[i], misc_send.at[5 + i], misc_recv.at[5 + i], where)

    order = flips[::-1] + ((0, 0),)
    sums = []
    for i, (fz, fx) in enumerate(order):
        zb_, x_ = flip(zb, fz), flip(x, fx)
        row = pl.multiple_of((zb_ * 2 + x_) * rows, rows)

        def down(j, carry, i=i, row=row):
            cols = pl.ds(pl.multiple_of(j * tile, tile), tile)
            v = jnp.dot(act[pl.ds(row, rows), :], wd[:, cols], preferred_element_type=F32)
            low, high = v[:half], v[half:]
            twin_out[i, :, cols] = jnp.where(t == 0, high, low).astype(BF16)
            part[:, cols] = jnp.where(t == 0, low, high)
            return carry

        with jax.named_scope("down"):
            lax.fori_loop(0, width // tile, down, 0)
        twin_copy(i).start()
        with jax.named_scope("twin_wait"):
            twin_copy(i).wait_recv()
        if i < 3:

            def add(r, carry, i=i):
                at = pl.ds(pl.multiple_of(r * 64, 64), 64)
                sum_out[i, at, :] = (part[at, :] + twin_in[i, at, :].astype(F32)).astype(BF16)
                return carry

            lax.fori_loop(0, half // 64, add, 0)
            c = sum_copy(i, (index(za, zb_, y, x_), t))
            c.start()
            sums.append(c)

    with jax.named_scope("sum_wait"):
        for i in range(3):
            sums[i].wait_recv()

    def last(r, carry):
        at = pl.ds(pl.multiple_of(r * 64, 64), 64)
        total = part[at, :] + twin_in[3, at, :].astype(F32)
        for i in range(3):
            total = total + sum_in[i, at, :].astype(F32)
        half_out[at, :] = (mid[at, :].astype(F32) + total).astype(BF16)
        return carry

    lax.fori_loop(0, half // 64, last, 0)
    final = remote(half_out, half_in, misc_send.at[0], misc_recv.at[0], (sp, u))
    final.start()
    out[pl.ds(pl.multiple_of(t * half, half), half), :] = half_out[...]
    with jax.named_scope("final_wait"):
        final.wait_recv()
    out[pl.ds(pl.multiple_of(u * half, half), half), :] = half_in[...]

    final.wait_send()
    for swap in swaps:
        swap.wait_send()

    @pl.when(sp < n_sp - 1)
    def _():
        for c in halo(0, (up_to, t)):
            c.wait_send()

    @pl.when(sp > 0)
    def _():
        for c in halo(1, (down_to, t)):
            c.wait_send()

    for w in range(2):
        for k in range(3):
            first_copy(w, k).wait_send()
        for c in sent[w]:
            c.wait_send()
    for r in range(rounds):
        for k in range(2):
            token_copy(k, r).wait_send()
        token_relay(r).wait_send()
        for k in range(4):
            pair_copy(k, t, r).wait_send()
    for i in range(4):
        twin_copy(i).wait_send()
    for c in sums:
        c.wait_send()


def extended(x, sides, width):
    for axis, dim in sides:
        count, length = (lax.axis_size(axis), x.shape[dim])
        up = [(i, (i + 1) % count) for i in range(count - 1)]
        down = [(j, i) for i, j in up]
        last = lax.slice_in_dim(x, length - width, length, axis=dim)
        initial = lax.slice_in_dim(x, 0, width, axis=dim)
        before = lax.ppermute(last, axis, up)
        after = lax.ppermute(initial, axis, down)
        x = jnp.concatenate([before, x, after], axis=dim)
    return x


def rms_scale(field, gain):
    wide = field.astype(jnp.float32)
    return wide * lax.rsqrt(jnp.mean(wide * wide, axis=-1, keepdims=True) + EPS) * gain


def mixer_partial(normed, w_up, w_down):
    upward = jnp.dot(
        normed, lax.all_gather(w_up, "sp", axis=0, tiled=True), preferred_element_type=jnp.float32
    )
    active = jnp.square(jax.nn.relu(upward)).astype(jnp.bfloat16)
    return jnp.dot(
        active, lax.all_gather(w_down, "sp", axis=1, tiled=True), preferred_element_type=jnp.float32
    )


def plain_shards(
    resid, queries, keys, values, documents, q_gain, k_gain, sink, w_out, n_gain, w_up, w_down
):
    rows = resid.shape[0]
    head_size = q_gain.shape[0]
    heads_here = sink.shape[0]
    kv_here = keys.shape[1] // head_size
    group = heads_here // kv_here
    qnorm = rms_scale(queries.reshape(rows, kv_here, group, head_size), q_gain).astype(jnp.bfloat16)
    knorm = rms_scale(keys.reshape(rows, kv_here, head_size), k_gain).astype(jnp.bfloat16)
    vheads = values.reshape(rows, kv_here, head_size)
    doc_here = documents.astype(jnp.bfloat16)
    near_keys, near_values, near_docs = (
        extended(knorm, (("sp", 0),), WINDOW),
        extended(vheads, (("sp", 0),), WINDOW),
        extended(doc_here, (("sp", 0),), WINDOW),
    )
    offset = lax.axis_index("sp") * rows
    total = rows * lax.axis_size("sp")
    query_pos = offset + jnp.arange(rows, dtype=jnp.int32)
    key_pos = offset - WINDOW + jnp.arange(rows + 2 * WINDOW, dtype=jnp.int32)
    distance = key_pos[None, :] - query_pos[:, None]
    allowed = (jnp.abs(distance) <= WINDOW) & (key_pos[None, :] >= 0) & (key_pos[None, :] < total)
    allowed = allowed & (near_docs[None, :] == doc_here[:, None])
    heads_all = heads_here * lax.axis_size("tp")
    first_head = (lax.axis_index("tp") * heads_here).astype(jnp.float32)
    slopes = jnp.exp2(
        -8.0 * (first_head + jnp.arange(heads_here, dtype=jnp.float32) + 1.0) / heads_all
    )
    slopes = slopes.reshape(kv_here, group)
    sink_f = sink.reshape(kv_here, group)
    scores = jnp.einsum(
        "rkgd,skd->kgrs", qnorm, near_keys, preferred_element_type=jnp.float32
    ) * head_size ** (-0.5)
    scores = scores - slopes[:, :, None, None] * jnp.abs(distance).astype(jnp.float32)[None, None]
    scores = jnp.where(allowed[None, None], scores, jnp.float32(-1e30))
    highest = jnp.maximum(jnp.max(scores, axis=-1), sink_f[:, :, None])
    weights = jnp.exp(scores - highest[..., None])
    denom = jnp.sum(weights, axis=-1) + jnp.exp(sink_f[:, :, None] - highest)
    summed = jnp.einsum(
        "kgrs,skd->rkgd",
        weights.astype(jnp.bfloat16),
        near_values,
        preferred_element_type=jnp.float32,
    )
    attended = (
        (summed / denom.transpose(2, 0, 1)[..., None])
        .astype(jnp.bfloat16)
        .reshape(rows, heads_here * head_size)
    )
    head_mix = lax.psum(
        jnp.dot(attended, w_out, preferred_element_type=jnp.float32).astype(jnp.bfloat16), "tp"
    ).astype(jnp.float32)
    middle = (resid.astype(jnp.float32) + head_mix).astype(jnp.bfloat16)
    normed = rms_scale(middle, n_gain).astype(jnp.bfloat16)
    partial_sum = mixer_partial(normed, w_up, w_down)
    unit_mix = lax.psum(partial_sum.astype(jnp.bfloat16), "tp").astype(jnp.float32)
    return (middle.astype(jnp.float32) + unit_mix).astype(jnp.bfloat16)


def fused_shards(
    resid, queries, keys, values, documents, q_gain, k_gain, sink, w_out, n_gain, w_up, w_down
):
    rows, width = resid.shape
    half = rows // 2
    n_sp = lax.axis_size("sp")
    head = q_gain.shape[0]
    heads = sink.shape[0]
    kv_heads = keys.shape[1] // head
    units = w_up.shape[1] // MEMBERS
    n_za = n_sp // 8
    rounds = half // WINDOW
    first = (lax.axis_index("tp") * heads).astype(F32)
    slopes = jnp.exp2(
        -8.0 * (first + jnp.arange(heads, dtype=F32) + 1.0) / (heads * lax.axis_size("tp"))
    )
    vmem = pl.BlockSpec(memory_space=pltpu.VMEM)
    smem = pl.BlockSpec(memory_space=pltpu.SMEM)
    hbm = pl.BlockSpec(memory_space=pl.ANY)
    sends = 3 + 4 * n_za + 4 * (n_za - 1)
    dma = pltpu.SemaphoreType.DMA
    return pl.pallas_call(
        functools.partial(kernel, n_sp, head, heads, kv_heads),
        out_shape=jax.ShapeDtypeStruct((rows, width), BF16),
        in_specs=[hbm, vmem, vmem, vmem, vmem, vmem, vmem, vmem, smem, smem, hbm, vmem, hbm, hbm],
        out_specs=vmem,
        scratch_shapes=[
            pltpu.VMEM((rows + 2 * WINDOW, keys.shape[1]), BF16),
            pltpu.VMEM((rows + 2 * WINDOW, keys.shape[1]), BF16),
            pltpu.VMEM((8, rows + 2 * WINDOW), jnp.int32),
            pltpu.VMEM((rows + 2 * WINDOW, keys.shape[1]), BF16),
            pltpu.VMEM((rows, heads * head), BF16),
            pltpu.VMEM(w_out.shape, BF16),
            pltpu.VMEM((half, width), BF16),
            pltpu.VMEM((rounds, WINDOW, width), BF16),
            pltpu.VMEM((rounds, WINDOW, width), BF16),
            pltpu.VMEM((rounds, WINDOW, width), BF16),
            pltpu.VMEM((half, width), BF16),
            pltpu.VMEM((MEMBERS * rows, width), BF16),
            pltpu.VMEM((width, units), BF16),
            pltpu.VMEM((units, width), BF16),
            pltpu.VMEM((MEMBERS * rows, units), BF16),
            pltpu.VMEM((half, width), F32),
            pltpu.VMEM((4, half, width), BF16),
            pltpu.VMEM((4, half, width), BF16),
            pltpu.VMEM((3, half, width), BF16),
            pltpu.VMEM((3, half, width), BF16),
            pltpu.VMEM((half, width), BF16),
            pltpu.VMEM((half, width), BF16),
            dma((2, 3)),
            dma((2, 3)),
            dma((2, sends)),
            dma((2, n_sp)),
            dma((2,)),
            dma((5,)),
            dma((3, rounds)),
            dma((3, rounds)),
            dma((4, rounds)),
            dma((4, rounds)),
            dma((rounds,)),
            dma((rounds,)),
            dma((8,)),
            dma((8,)),
        ],
        compiler_params=pltpu.CompilerParams(
            collective_id=0, has_side_effects=True, vmem_limit_bytes=62 * 1024 * 1024
        ),
        name="layer",
    )(
        resid,
        queries,
        keys,
        values,
        documents[:, None],
        jnp.broadcast_to(documents[None, :], (8, rows)),
        q_gain[None, :],
        k_gain[None, :],
        slopes,
        sink,
        w_out,
        n_gain[None, :],
        w_up,
        w_down,
    )


def solution(mesh):
    placed = (
        P("sp", None),
        P("sp", "tp"),
        P("sp", "tp"),
        P("sp", "tp"),
        P("sp"),
        P(),
        P(),
        P("tp"),
        P("tp", None),
        P(),
        P("sp", "tp"),
        P("tp", "sp"),
    )
    sizes = dict(mesh.shape)

    def shards(*args):
        columns = args[11].shape[1]
        fits = sizes["tp"] == 2 and sizes["sp"] % 8 == 0 and columns % 128 == 0
        return (fused_shards if fits else plain_shards)(*args)

    return jax.shard_map(
        shards, mesh=mesh, in_specs=placed, out_specs=P("sp", None), check_vma=False
    )
```

profile of v0, /device:TPU:13, one launch (start us, length us, event | category | flops | bytes accessed | tf_op | source)
XLA Modules:
  0.0 180.9 jit_solution(3434733062447273961)
XLA Ops:
  0.0 0.6 multiply_exponential_fusion.slopes
  0.6 1.3 broadcast_in_dim.19.doc_row
  1.8 1.5 copy.13.doc_col
  3.4 174.4 %layer.1 = bf16[512,2048]{1,0:T(8,128)(2,1)} custom-call(bf16[512,2048]{1,0:T(8,128)(2,1)} %resid.1, bf16[512,1024]{1,0:T(8,128)(2,1)} %queries.1, bf16[512,256]{1,0:T(8,128)(2,1)} %keys.1, bf16[512,256]{1,0:T(8,128)(2,1)} %values.1, s32[512,1]{1,0:T(8,128)} %copy.13.doc_col, s32[8,512]{1,0:T(8,128)} %broadcast_in_dim.19.doc_row, f32[1,64]{1,0:T(1,128)} %bitcast.6, ...), custom_call_target="tpu_custom_call" | custom-call | tf_op jit(solution)/shard_map/layer/pallas_call | solution.py:626
  177.8 3.2 %copy.15 = bf16[512,2048]{1,0:T(8,128)(2,1)} copy(bf16[512,2048]{1,0:T(8,128)(2,1)} %layer.1) | data formatting | bytes 4194304
where the time goes:
time: 182 us; the launch traced here: 181 us
  Pallas kernels  174 us (96%)
  local copies, waits for them, and re-layouts  5.97 us (3%)
    pallas_call x1, Pallas kernels, fused_shards(): pl.pallas_call(functools.partial(kernel, n_sp, head, heads, kv_heads), ou...  174 us

commit v1 on v0

v1 whole, which is shorter than its diff:
```python
import functools

import jax
import jax.numpy as jnp
from jax import lax
from jax.experimental import pallas as pl
from jax.experimental.pallas import tpu as pltpu
from jax.sharding import PartitionSpec as P

WINDOW = 128
EPS = 1e-06
MEMBERS = 4
F32 = jnp.float32
BF16 = jnp.bfloat16
MESH = pl.DeviceIdType.MESH


def rms(wide, gain):
    return wide * lax.rsqrt(jnp.mean(wide * wide, axis=-1, keepdims=True) + EPS) * gain


def kernel(
    n_sp,
    head,
    heads,
    kv_heads,
    slopes,
    resid,
    queries,
    keys,
    values,
    docs,
    q_gain,
    k_gain,
    sink,
    w_out,
    n_gain,
    w_up,
    w_down,
    out,
    q,
    kx,
    vx,
    dx,
    kn,
    att,
    wo,
    res,
    mixed,
    other_in,
    mid,
    normed,
    wu,
    wd,
    act,
    part,
    twin_out,
    twin_in,
    first_out,
    first_in,
    second_out,
    second_in,
    waiting,
    total,
    half_out,
    halo_send,
    halo_recv,
    w_send,
    w_recv,
    w_local,
    loc_sem,
    tok_send,
    tok_recv,
    pair_send,
    pair_recv,
    swap_send,
    swap_recv,
    twin_send,
    twin_recv,
    sum_send,
    sum_recv,
    fin_send,
    fin_recv,
    fin_local,
):
    rows = queries.shape[0]
    half = rows // 2
    depth = w_up.shape[0]
    units = wu.shape[1]
    width = wd.shape[1]
    group = heads // kv_heads
    n_za = n_sp // 8
    block = 2 * w_down.shape[1]

    sp = lax.axis_index("sp")
    t = lax.axis_index("tp")
    u = 1 - t
    x = sp % 2
    y = (sp // 2) % 2
    zb = (sp // 4) % 2
    za = sp // 8
    me = zb * 2 + x

    def index(za_, zb_, y_, x_):
        return za_ * 8 + zb_ * 4 + y_ * 2 + x_

    def flip(v, by):
        return 1 - v if by else v

    def remote(src, dst, send, recv, where):
        return pltpu.make_async_remote_copy(
            src_ref=src, dst_ref=dst, send_sem=send, recv_sem=recv,
            device_id=where, device_id_type=MESH,
        )

    own_q = pltpu.make_async_copy(queries, q, loc_sem.at[5])
    own_k = pltpu.make_async_copy(keys, kx.at[pl.ds(WINDOW, rows), :], loc_sem.at[2])
    own_v = pltpu.make_async_copy(values, vx.at[pl.ds(WINDOW, rows), :], loc_sem.at[3])
    own_d = pltpu.make_async_copy(docs, dx.at[:, pl.ds(WINDOW, rows)], loc_sem.at[4])
    own_k.start()
    own_d.start()
    own_q.start()
    own_v.start()

    up_to = lax.rem(sp + 1, n_sp)
    down_to = lax.rem(sp + n_sp - 1, n_sp)
    flips = ((0, 1), (1, 0), (1, 1))
    near = [(index(za, flip(zb, fz), y, flip(x, fx)), t) for fz, fx in flips]
    across = (index(za, zb, 1 - y, x), t)
    partners = [(sp, u), (up_to, t), (down_to, t), across] + near
    partners += [(index(lax.rem(za + d, n_za), zb, y, x), t) for d in range(1, n_za)]
    with jax.named_scope("barrier"):
        greeting = pltpu.get_barrier_semaphore()
        for where in partners:
            pl.semaphore_signal(greeting, inc=1, device_id=where, device_id_type=MESH)
        pl.semaphore_wait(greeting, len(partners))

    def halo(side, where):
        src = rows - WINDOW if side == 0 else 0
        dst = 0 if side == 0 else WINDOW + rows
        return [
            remote(keys.at[pl.ds(src, WINDOW), :], kx.at[pl.ds(dst, WINDOW), :],
                   halo_send.at[side, 0], halo_recv.at[side, 0], where),
            remote(docs.at[:, pl.ds(src, WINDOW)], dx.at[:, pl.ds(dst, WINDOW)],
                   halo_send.at[side, 2], halo_recv.at[side, 2], where),
            remote(values.at[pl.ds(src, WINDOW), :], vx.at[pl.ds(dst, WINDOW), :],
                   halo_send.at[side, 1], halo_recv.at[side, 1], where),
        ]

    @pl.when(sp < n_sp - 1)
    def _():
        for c in halo(0, (up_to, t)):
            c.start()

    @pl.when(sp > 0)
    def _():
        for c in halo(1, (down_to, t)):
            c.start()

    def place(w, s):
        if w == 0:
            return wu.at[pl.ds(pl.multiple_of(s * depth, depth), depth), :]
        return wd.at[:, pl.ds(pl.multiple_of(s * (block // 2), block // 2), block // 2)]

    def source(w, m):
        at = pl.ds(pl.multiple_of(m * units, units), units)
        return w_up.at[:, at] if w == 0 else w_down.at[at, :]

    def first_copy(w, k):
        fz, fx = flips[k]
        return remote(source(w, flip(zb, fz) * 2 + flip(x, fx)), place(w, sp), w_send.at[w, k],
                      w_recv.at[w, sp], near[k])

    locals_ = [pltpu.make_async_copy(source(w, me), place(w, sp), w_local.at[w]) for w in range(2)]

    def arrived(w, s):
        remote(place(w, s), place(w, s), w_send.at[w, 0], w_recv.at[w, s], (sp, u)).wait_recv()

    sent = [[], []]

    def start(w, s, where, src=None):
        c = remote(place(w, s) if src is None else src, place(w, s), w_send.at[w, 3 + len(sent[w])],
                   w_recv.at[w, s], where)
        c.start()
        sent[w].append(c)

    def along(w, s, src=None):
        for d in range(1, n_za):
            start(w, s, (index(lax.rem(za + d, n_za), zb, y, x), t), src)

    def member_at(k):
        fz, fx = (0, 0) if k == 0 else flips[k - 1]
        return flip(zb, fz), flip(x, fx)

    def spread(w, k):
        with jax.named_scope(f"spread#w={w}#k={k}"):
            zb_, x_ = member_at(k)
            s = index(za, zb_, y, x_)
            arrived(w, s)
            along(w, s)

    def cross(w, k):
        zb_, x_ = member_at(k)
        start(w, index(za, zb_, y, x_), across, source(w, me) if k == 0 else None)

    def relay(w, k):
        with jax.named_scope(f"relay#w={w}#k={k}"):
            zb_, x_ = member_at(k)
            for d in range(1, n_za):
                s = index(lax.rem(za + n_za - d, n_za), zb_, y, x_)
                arrived(w, s)
                start(w, s, across)

    def exchange(w):
        for k in (1, 2, 0):
            first_copy(w, k).start()
        locals_[w].start()

    exchange(0)
    along(0, sp, source(0, me))
    cross(0, 0)
    exchange(1)
    load_wo = pltpu.make_async_copy(w_out, wo, loc_sem.at[0])
    load_wo.start()
    load_res = pltpu.make_async_copy(resid.at[pl.ds(t * half, half), :], res, loc_sem.at[1])
    load_res.start()

    with jax.named_scope("own_wait"):
        own_k.wait()
        own_v.wait()
        own_d.wait()
        own_q.wait()

    @pl.when(sp > 0)
    def _():
        for c in halo(0, (down_to, t)):
            c.wait_recv()

    @pl.when(sp == 0)
    def _():
        kx[pl.ds(0, WINDOW), :] = jnp.zeros((WINDOW, kx.shape[1]), BF16)
        vx[pl.ds(0, WINDOW), :] = jnp.zeros((WINDOW, vx.shape[1]), BF16)
        dx[:, pl.ds(0, WINDOW)] = jnp.full((1, WINDOW), -1, jnp.int32)

    @pl.when(sp < n_sp - 1)
    def _():
        for c in halo(1, (up_to, t)):
            c.wait_recv()

    @pl.when(sp == n_sp - 1)
    def _():
        end = WINDOW + rows
        kx[pl.ds(end, WINDOW), :] = jnp.zeros((WINDOW, kx.shape[1]), BF16)
        vx[pl.ds(end, WINDOW), :] = jnp.zeros((WINDOW, vx.shape[1]), BF16)
        dx[:, pl.ds(end, WINDOW)] = jnp.full((1, WINDOW), -1, jnp.int32)

    def norm_keys(b, carry):
        at = pl.ds(pl.multiple_of(b * WINDOW, WINDOW), WINDOW)
        wide = kx[at, :].astype(F32)
        kn[at, :] = jnp.concatenate(
            [rms(wide[:, k * head:(k + 1) * head], k_gain[...]) for k in range(kv_heads)], axis=1
        ).astype(BF16)
        return carry

    with jax.named_scope("norm_keys"):
        lax.fori_loop(0, kx.shape[0] // WINDOW, norm_keys, 0)

    span = 3 * WINDOW
    rounds = half // WINDOW

    def attend(b, carry, to):
        at = pl.ds(pl.multiple_of(b * WINDOW, WINDOW), WINDOW)
        put = pl.ds(pl.multiple_of(to * WINDOW, WINDOW), WINDOW)
        window = pl.ds(pl.multiple_of(b * WINDOW, WINDOW), span)
        far = jnp.abs(
            lax.broadcasted_iota(jnp.int32, (WINDOW, span), 1)
            - lax.broadcasted_iota(jnp.int32, (WINDOW, span), 0) - WINDOW
        )
        own = dx[0:1, pl.ds(pl.multiple_of((b + 1) * WINDOW, WINDOW), WINDOW)].astype(F32)
        own = jnp.transpose(jnp.broadcast_to(own, (WINDOW, WINDOW)))[:, 0:1]
        allowed = (far <= WINDOW) & (dx[0:1, window].astype(F32) == own)
        mask = jnp.where(allowed, F32(0.0), F32(-1e30))
        far = far.astype(F32)
        for k in range(kv_heads):
            lanes = slice(k * head, (k + 1) * head)
            kb = kn[window, lanes]
            vb = vx[window, lanes]
            done = []
            for g in range(group):
                h = k * group + g
                slope = jnp.where(t == 0, F32(slopes[h]), F32(slopes[heads + h]))
                qb = rms(q[at, h * head:(h + 1) * head].astype(F32), q_gain[...]).astype(BF16)
                score = lax.dot_general(
                    qb, kb, (((1,), (1,)), ((), ())), preferred_element_type=F32
                ) * (head ** -0.5)
                score = (score - slope * far) + mask
                top = jnp.maximum(jnp.max(score, axis=-1, keepdims=True), sink[h])
                p = jnp.exp(score - top)
                denom = jnp.sum(p, axis=-1, keepdims=True) + jnp.exp(sink[h] - top)
                summed = jnp.dot(p.astype(BF16), vb, preferred_element_type=F32)
                done.append((summed / denom).astype(BF16))
                if len(done) == 2:
                    att[put, (h - 1) * head:(h + 1) * head] = jnp.concatenate(done, axis=1)
                    done = []
        return carry

    tile = 256
    swaps = []

    def project(r):
        lhs = att[pl.ds(r * 2 * WINDOW, 2 * WINDOW), :]

        def step(j, carry):
            cols = pl.ds(pl.multiple_of(j * tile, tile), tile)
            mixed[r, :, cols] = jnp.dot(lhs, wo[:, cols], preferred_element_type=F32).astype(BF16)
            return carry

        lax.fori_loop(0, width // tile, step, 0)

    def token_rows(slot, r):
        return normed.at[pl.ds(pl.multiple_of(slot * half + r * WINDOW, WINDOW), WINDOW), :]

    def token_copy(k, r):
        rows_ = token_rows(me * 2 + t, r)
        return remote(rows_, rows_, tok_send.at[k, r], tok_recv.at[k, r], near[k])

    def member(k):
        if k == 3:
            return me
        fz, fx = flips[k]
        return flip(zb, fz) * 2 + flip(x, fx)

    def pair_copy(k, core, r):
        rows_ = token_rows(member(k) * 2 + core, r)
        return remote(rows_, rows_, pair_send.at[k, r], pair_recv.at[k, r], (sp, u))

    def token_pass(k, r):
        with jax.named_scope(f"token#k={k}#r={r}"):
            rows_ = token_rows(member(k) * 2 + t, r)
            remote(rows_, rows_, tok_send.at[k, r], tok_recv.at[k, r], (sp, u)).wait_recv()
            if k == 1:
                token_relay(r).start()
            pair_copy(k, t, r).start()

    def token_relay(r):
        rows_ = token_rows(member(1) * 2 + t, r)
        return remote(rows_, rows_, tok_send.at[2, r], tok_recv.at[2, r], near[0])

    def one_round(r):
        with jax.named_scope("project"):
            project(r)
            swap = remote(mixed.at[r, pl.ds(pl.multiple_of(u * WINDOW, WINDOW), WINDOW), :], other_in.at[r],
                          swap_send.at[r], swap_recv.at[r], (sp, u))
            swap.start()
            swaps.append(swap)
        with jax.named_scope("swap_wait"):
            swap.wait_recv()

        def middle(i, carry):
            at = pl.ds(pl.multiple_of(i * 64, 64), 64)
            mine = pl.ds(pl.multiple_of(t * WINDOW + i * 64, 64), 64)
            here = pl.ds(pl.multiple_of(r * WINDOW + i * 64, 64), 64)
            both = mixed[r, mine, :].astype(F32) + other_in[r, at, :].astype(F32)
            value = (res[here, :].astype(F32) + both).astype(BF16)
            mid[here, :] = value
            row = pl.multiple_of((me * 2 + t) * half + r * WINDOW + i * 64, 64)
            normed[pl.ds(row, 64), :] = rms(value.astype(F32), n_gain[...]).astype(BF16)
            return carry

        with jax.named_scope("middle"):
            lax.fori_loop(0, WINDOW // 64, middle, 0)
        for k in (1, 0):
            token_copy(k, r).start()
        pair_copy(3, t, r).start()

    def attend_block(r, i):
        with jax.named_scope("attend"):
            lax.fori_loop(0, 1, lambda _, c: attend(r + i * rounds, c, 2 * r + i), 0)

    for r in range(rounds):
        attend_block(r, 0)
        if r == 0:
            spread(0, 1)
            cross(0, 1)
        attend_block(r, 1)
        if r == 0:
            for k in (2, 3):
                spread(0, k)
                cross(0, k)
            load_wo.wait()
            load_res.wait()
        one_round(r)

    def up(m):
        row = pl.multiple_of(m * rows, rows)

        def step(j, carry):
            cols = pl.ds(pl.multiple_of(j * tile, tile), tile)
            v = jnp.dot(normed[pl.ds(row, rows), :], wu[:, cols], preferred_element_type=F32)
            v = jnp.maximum(v, 0.0)
            act[pl.ds(row, rows), cols] = (v * v).astype(BF16)
            return carry

        with jax.named_scope("up"):
            lax.fori_loop(0, units // tile, step, 0)

    def pair_wait(k):
        with jax.named_scope("pair_wait"):
            for r in range(rounds):
                pair_copy(k, u, r).wait_recv()

    def finish_up():
        with jax.named_scope("finish_up"):
            locals_[0].wait()
            for a in range(n_za):
                for k in range(4):
                    arrived(0, index(a, k // 2, 1 - y, k % 2))

    along(1, sp, source(1, me))
    for k in (1, 2, 3):
        spread(1, k)
    for k in range(4):
        relay(0, k)
    for k in range(4):
        cross(1, k)
    for r in range(rounds):
        token_pass(1, r)
    finish_up()
    pair_wait(3)
    up(me)
    for r in range(rounds):
        token_pass(0, r)
    pair_wait(0)
    up(member(0))
    for r in range(rounds):
        token_pass(2, r)
    relay(1, 0)
    relay(1, 1)
    for k in (1, 2):
        pair_wait(k)
        up(member(k))
    locals_[1].wait()

    order = [(d, fz, fy) for d in range(n_za) for fy in range(2) for fz in range(2)]
    chunks = 4
    ways = ((0, 1), (1, 0))

    def block_of(p):
        d, fz, fy = order[p]
        return lax.rem(za + n_za - d, n_za) * 4 + flip(zb, fz) * 2 + flip(y, fy)

    def axes(p):
        return ways[0] if order[p][0] % 2 == 0 else ways[1]

    def cols_of(g):
        return pl.ds(pl.multiple_of(g * block, block), block)

    def twin_copy(g):
        return remote(twin_out.at[g], twin_in.at[g], twin_send.at[g], twin_recv.at[g], (sp, u))

    def first_sum(p):
        g = block_of(p)
        return remote(first_out.at[g], first_in.at[g], sum_send.at[0, g], sum_recv.at[0, g], near[axes(p)[0]])

    def second_sum(p):
        g = block_of(p)
        return remote(second_out.at[g], second_in.at[g], sum_send.at[1, g], sum_recv.at[1, g], near[axes(p)[1]])

    def down(p):
        d, fz, fy = order[p]
        g = block_of(p)
        with jax.named_scope(f"down_wait#p={p}"):
            if fy == 1:
                for i in range(2):
                    arrived(1, g * 2 + i)
        cols = cols_of(g)

        def step(c, carry):
            cz, cx = c // 2, c % 2
            row = (zb + cz - 2 * zb * cz) * 2 + (x + cx - 2 * x * cx)
            theirs = pl.ds(pl.multiple_of(row * rows + u * half, half), half)
            ours = pl.ds(pl.multiple_of(row * rows + t * half, half), half)
            twin_out[g, c, :, :] = jnp.dot(act[theirs, :], wd[:, cols], preferred_element_type=F32).astype(BF16)
            part[p % 2, c, :, :] = jnp.dot(act[ours, :], wd[:, cols], preferred_element_type=F32)
            return carry

        with jax.named_scope("down"):
            lax.fori_loop(0, chunks, step, 0)
        twin_copy(g).start()

    def combine(p):
        g = block_of(p)
        cols = cols_of(g)
        one, two = axes(p)
        with jax.named_scope("twin_wait"):
            twin_copy(g).wait_recv()

        def add(i, carry):
            at = pl.ds(pl.multiple_of(i * 64, 64), 64)

            def whole(c):
                return part[p % 2, c, at, :] + twin_in[g, c, at, :].astype(F32)

            first_out[g, 0, at, :] = whole(3).astype(BF16)
            first_out[g, 1, at, :] = whole(one + 1).astype(BF16)
            waiting[g, at, :] = whole(two + 1)
            total[g, at, :] = whole(0) + mid[at, cols].astype(F32)
            return carry

        with jax.named_scope("combine"):
            lax.fori_loop(0, half // 64, add, 0)
        first_sum(p).start()

    def merge(p):
        g = block_of(p)
        with jax.named_scope(f"merge_wait#p={p}"):
            first_sum(p).wait_recv()

        def add(i, carry):
            at = pl.ds(pl.multiple_of(i * 64, 64), 64)
            second_out[g, at, :] = (waiting[g, at, :] + first_in[g, 0, at, :].astype(F32)).astype(BF16)
            return carry

        lax.fori_loop(0, half // 64, add, 0)
        second_sum(p).start()

    def final_copies(p):
        g = block_of(p)
        cols = cols_of(g)
        mine = pl.ds(pl.multiple_of(t * half, half), half)
        return (
            pltpu.make_async_copy(half_out.at[g], out.at[mine, cols], fin_local.at[g]),
            remote(half_out.at[g], out.at[mine, cols], fin_send.at[g], fin_recv.at[g], (sp, u)),
        )

    def last(p):
        g = block_of(p)
        with jax.named_scope(f"sum_wait#p={p}"):
            second_sum(p).wait_recv()

        def add(i, carry):
            at = pl.ds(pl.multiple_of(i * 64, 64), 64)
            value = total[g, at, :] + first_in[g, 1, at, :].astype(F32) + second_in[g, at, :].astype(F32)
            half_out[g, at, :] = value.astype(BF16)
            return carry

        lax.fori_loop(0, half // 64, add, 0)
        for c in final_copies(p):
            c.start()

    count = len(order)
    for p in range(count + 3):
        if p < count:
            if p == 2:
                relay(1, 2)
            if p == 3:
                relay(1, 3)
            down(p)
        if 1 <= p <= count:
            combine(p - 1)
        if 3 <= p:
            merge(p - 3)
    for p in range(count):
        last(p)
    with jax.named_scope("final_wait"):
        for p in range(count):
            here, there = final_copies(p)
            here.wait()
            there.wait()

    for swap in swaps:
        swap.wait_send()

    @pl.when(sp < n_sp - 1)
    def _():
        for c in halo(0, (up_to, t)):
            c.wait_send()

    @pl.when(sp > 0)
    def _():
        for c in halo(1, (down_to, t)):
            c.wait_send()

    for w in range(2):
        for k in range(3):
            first_copy(w, k).wait_send()
        for c in sent[w]:
            c.wait_send()
    for r in range(rounds):
        for k in range(2):
            token_copy(k, r).wait_send()
        token_relay(r).wait_send()
        for k in range(4):
            pair_copy(k, t, r).wait_send()
    for p in range(count):
        twin_copy(block_of(p)).wait_send()
        first_sum(p).wait_send()
        second_sum(p).wait_send()


def extended(x, sides, width):
    for axis, dim in sides:
        count, length = (lax.axis_size(axis), x.shape[dim])
        up = [(i, (i + 1) % count) for i in range(count - 1)]
        down = [(j, i) for i, j in up]
        last = lax.slice_in_dim(x, length - width, length, axis=dim)
        initial = lax.slice_in_dim(x, 0, width, axis=dim)
        before = lax.ppermute(last, axis, up)
        after = lax.ppermute(initial, axis, down)
        x = jnp.concatenate([before, x, after], axis=dim)
    return x


def rms_scale(field, gain):
    wide = field.astype(jnp.float32)
    return wide * lax.rsqrt(jnp.mean(wide * wide, axis=-1, keepdims=True) + EPS) * gain


def mixer_partial(normed, w_up, w_down):
    upward = jnp.dot(
        normed, lax.all_gather(w_up, "sp", axis=0, tiled=True), preferred_element_type=jnp.float32
    )
    active = jnp.square(jax.nn.relu(upward)).astype(jnp.bfloat16)
    return jnp.dot(
        active, lax.all_gather(w_down, "sp", axis=1, tiled=True), preferred_element_type=jnp.float32
    )


def plain_shards(
    resid, queries, keys, values, documents, q_gain, k_gain, sink, w_out, n_gain, w_up, w_down
):
    rows = resid.shape[0]
    head_size = q_gain.shape[0]
    heads_here = sink.shape[0]
    kv_here = keys.shape[1] // head_size
    group = heads_here // kv_here
    qnorm = rms_scale(queries.reshape(rows, kv_here, group, head_size), q_gain).astype(jnp.bfloat16)
    knorm = rms_scale(keys.reshape(rows, kv_here, head_size), k_gain).astype(jnp.bfloat16)
    vheads = values.reshape(rows, kv_here, head_size)
    doc_here = documents.astype(jnp.bfloat16)
    near_keys, near_values, near_docs = (
        extended(knorm, (("sp", 0),), WINDOW),
        extended(vheads, (("sp", 0),), WINDOW),
        extended(doc_here, (("sp", 0),), WINDOW),
    )
    offset = lax.axis_index("sp") * rows
    total = rows * lax.axis_size("sp")
    query_pos = offset + jnp.arange(rows, dtype=jnp.int32)
    key_pos = offset - WINDOW + jnp.arange(rows + 2 * WINDOW, dtype=jnp.int32)
    distance = key_pos[None, :] - query_pos[:, None]
    allowed = (jnp.abs(distance) <= WINDOW) & (key_pos[None, :] >= 0) & (key_pos[None, :] < total)
    allowed = allowed & (near_docs[None, :] == doc_here[:, None])
    heads_all = heads_here * lax.axis_size("tp")
    first_head = (lax.axis_index("tp") * heads_here).astype(jnp.float32)
    slopes = jnp.exp2(
        -8.0 * (first_head + jnp.arange(heads_here, dtype=jnp.float32) + 1.0) / heads_all
    )
    slopes = slopes.reshape(kv_here, group)
    sink_f = sink.reshape(kv_here, group)
    scores = jnp.einsum(
        "rkgd,skd->kgrs", qnorm, near_keys, preferred_element_type=jnp.float32
    ) * head_size ** (-0.5)
    scores = scores - slopes[:, :, None, None] * jnp.abs(distance).astype(jnp.float32)[None, None]
    scores = jnp.where(allowed[None, None], scores, jnp.float32(-1e30))
    highest = jnp.maximum(jnp.max(scores, axis=-1), sink_f[:, :, None])
    weights = jnp.exp(scores - highest[..., None])
    denom = jnp.sum(weights, axis=-1) + jnp.exp(sink_f[:, :, None] - highest)
    summed = jnp.einsum(
        "kgrs,skd->rkgd",
        weights.astype(jnp.bfloat16),
        near_values,
        preferred_element_type=jnp.float32,
    )
    attended = (
        (summed / denom.transpose(2, 0, 1)[..., None])
        .astype(jnp.bfloat16)
        .reshape(rows, heads_here * head_size)
    )
    head_mix = lax.psum(
        jnp.dot(attended, w_out, preferred_element_type=jnp.float32).astype(jnp.bfloat16), "tp"
    ).astype(jnp.float32)
    middle = (resid.astype(jnp.float32) + head_mix).astype(jnp.bfloat16)
    normed = rms_scale(middle, n_gain).astype(jnp.bfloat16)
    partial_sum = mixer_partial(normed, w_up, w_down)
    unit_mix = lax.psum(partial_sum.astype(jnp.bfloat16), "tp").astype(jnp.float32)
    return (middle.astype(jnp.float32) + unit_mix).astype(jnp.bfloat16)


def fused_shards(
    resid, queries, keys, values, documents, q_gain, k_gain, sink, w_out, n_gain, w_up, w_down
):
    rows, width = resid.shape
    half = rows // 2
    n_sp = lax.axis_size("sp")
    head = q_gain.shape[0]
    heads = sink.shape[0]
    kv_heads = keys.shape[1] // head
    units = w_up.shape[1] // MEMBERS
    n_za = n_sp // 8
    rounds = half // WINDOW
    heads_all = heads * lax.axis_size("tp")
    slopes = tuple(2.0 ** (-8.0 * (h + 1.0) / heads_all) for h in range(heads_all))
    vmem = pl.BlockSpec(memory_space=pltpu.VMEM)
    smem = pl.BlockSpec(memory_space=pltpu.SMEM)
    hbm = pl.BlockSpec(memory_space=pl.ANY)
    sends = 3 + 4 * n_za + 4 * (n_za - 1)
    block = 2 * w_down.shape[1]
    blocks = width // block
    dma = pltpu.SemaphoreType.DMA
    return pl.pallas_call(
        functools.partial(kernel, n_sp, head, heads, kv_heads, slopes),
        out_shape=jax.ShapeDtypeStruct((rows, width), BF16),
        in_specs=[hbm, hbm, hbm, hbm, hbm, vmem, vmem, smem, hbm, vmem, hbm, hbm],
        out_specs=hbm,
        scratch_shapes=[
            pltpu.VMEM((rows, heads * head), BF16),
            pltpu.VMEM((rows + 2 * WINDOW, keys.shape[1]), BF16),
            pltpu.VMEM((rows + 2 * WINDOW, keys.shape[1]), BF16),
            pltpu.VMEM((1, rows + 2 * WINDOW), jnp.int32),
            pltpu.VMEM((rows + 2 * WINDOW, keys.shape[1]), BF16),
            pltpu.VMEM((rows, heads * head), BF16),
            pltpu.VMEM(w_out.shape, BF16),
            pltpu.VMEM((half, width), BF16),
            pltpu.VMEM((rounds, 2 * WINDOW, width), BF16),
            pltpu.VMEM((rounds, WINDOW, width), BF16),
            pltpu.VMEM((half, width), BF16),
            pltpu.VMEM((MEMBERS * rows, width), BF16),
            pltpu.VMEM((width, units), BF16),
            pltpu.VMEM((units, width), BF16),
            pltpu.VMEM((MEMBERS * rows, units), BF16),
            pltpu.VMEM((2, MEMBERS, half, block), F32),
            pltpu.VMEM((blocks, MEMBERS, half, block), BF16),
            pltpu.VMEM((blocks, MEMBERS, half, block), BF16),
            pltpu.VMEM((blocks, 2, half, block), BF16),
            pltpu.VMEM((blocks, 2, half, block), BF16),
            pltpu.VMEM((blocks, half, block), BF16),
            pltpu.VMEM((blocks, half, block), BF16),
            pltpu.VMEM((blocks, half, block), F32),
            pltpu.VMEM((blocks, half, block), F32),
            pltpu.VMEM((blocks, half, block), BF16),
            dma((2, 3)),
            dma((2, 3)),
            dma((2, sends)),
            dma((2, n_sp)),
            dma((2,)),
            dma((6,)),
            dma((3, rounds)),
            dma((3, rounds)),
            dma((4, rounds)),
            dma((4, rounds)),
            dma((rounds,)),
            dma((rounds,)),
            dma((blocks,)),
            dma((blocks,)),
            dma((2, blocks)),
            dma((2, blocks)),
            dma((blocks,)),
            dma((blocks,)),
            dma((blocks,)),
        ],
        compiler_params=pltpu.CompilerParams(
            collective_id=0, has_side_effects=True, vmem_limit_bytes=63 * 1024 * 1024
        ),
        name="layer",
    )(
        resid,
        queries,
        keys,
        values,
        documents[None, :],
        q_gain[None, :],
        k_gain[None, :],
        sink,
        w_out,
        n_gain[None, :],
        w_up,
        w_down,
    )


def solution(mesh):
    placed = (
        P("sp", None),
        P("sp", "tp"),
        P("sp", "tp"),
        P("sp", "tp"),
        P("sp"),
        P(),
        P(),
        P("tp"),
        P("tp", None),
        P(),
        P("sp", "tp"),
        P("tp", "sp"),
    )
    sizes = dict(mesh.shape)

    def shards(*args):
        columns = args[11].shape[1]
        fits = sizes["tp"] == 2 and sizes["sp"] % 8 == 0 and columns % 128 == 0
        return (fused_shards if fits else plain_shards)(*args)

    return jax.shard_map(
        shards, mesh=mesh, in_specs=placed, out_specs=P("sp", None), check_vma=False
    )
```

time: 182 us -> 173 us (0.951)
  Pallas kernels: 174 us -> 168 us
  local copies, waits for them, and re-layouts: 5.97 us -> 3.16 us
    pallas_call x1, Pallas kernels: 174 us -> 168 us  [fused_shards(): pl.pallas_call(functools.partial(kernel, n_sp, head, heads, kv_heads, slo...]
    broadcast_in_dim x2 -> x0, local copies, waits for them, and re-layouts: 2.81 us -> none  [the longest x1 1.53 us: fused_shards(): documents[:, None]]
where the time goes in v1:
time: 173 us; the launch traced here: 171 us
  Pallas kernels  168 us (97%)
  local copies, waits for them, and re-layouts  3.16 us (2%)
    pallas_call x1, Pallas kernels, fused_shards(): pl.pallas_call(functools.partial(kernel, n_sp, head, heads, kv_heads, slo...  168 us

profile of v1, /device:TPU:13, one launch (start us, length us, event | category | flops | bytes accessed | tf_op | source)
XLA Modules:
  0.0 170.7 jit_solution(10512773687328666311)
XLA Ops:
  0.0 167.6 %layer.1 = bf16[512,2048]{1,0:T(8,128)(2,1)} custom-call(bf16[512,2048]{1,0:T(8,128)(2,1)} %resid.1, bf16[512,1024]{1,0:T(8,128)(2,1)} %queries.1, bf16[512,256]{1,0:T(8,128)(2,1)} %keys.1, bf16[512,256]{1,0:T(8,128)(2,1)} %values.1, s32[1,512]{1,0:T(1,128)} %bitcast.5, f32[1,64]{1,0:T(1,128)} %bitcast.6, f32[1,64]{1,0:T(1,128)} %bitcast.7, f32[16]{0:T(128)} %sink.1, ...), custom_call_target="tpu_custom_call" | custom-call | tf_op jit(solution)/shard_map/layer/pallas_call | solution.py:710
  167.6 3.2 %copy.14 = bf16[512,2048]{1,0:T(8,128)(2,1)} copy(bf16[512,2048]{1,0:T(8,128)(2,1)} %layer.1) | data formatting | bytes 4194304

commit v2 on v1

--- a/solution.py
+++ b/solution.py
@@ -82,6 +82,7 @@
     fin_send,
     fin_recv,
     fin_local,
+    credit,
 ):
     rows = queries.shape[0]
     half = rows // 2
@@ -128,7 +129,9 @@
     near = [(index(za, flip(zb, fz), y, flip(x, fx)), t) for fz, fx in flips]
     across = (index(za, zb, 1 - y, x), t)
     partners = [(sp, u), (up_to, t), (down_to, t), across] + near
-    partners += [(index(lax.rem(za + d, n_za), zb, y, x), t) for d in range(1, n_za)]
+    partners += [(index(1 - za, zb_, y, x_), t) for zb_, x_ in ((zb, x), (1 - zb, x), (1 - zb, 1 - x))]
+    opposite = partners[-3:]
+    inner = za + zb == 1
     with jax.named_scope("barrier"):
         greeting = pltpu.get_barrier_semaphore()
         for where in partners:
@@ -178,27 +181,31 @@
 
     sent = [[], []]
 
-    def start(w, s, where, src=None):
+    def start(w, s, where, src=None, only=None):
         c = remote(place(w, s) if src is None else src, place(w, s), w_send.at[w, 3 + len(sent[w])],
                    w_recv.at[w, s], where)
-        c.start()
-        sent[w].append(c)
-
-    def along(w, s, src=None):
-        for d in range(1, n_za):
-            start(w, s, (index(lax.rem(za + d, n_za), zb, y, x), t), src)
+        if only is None:
+            c.start()
+        else:
+            pl.when(only)(c.start)
+        sent[w].append((c, only))
+
+    def direct(w, i):
+        start(w, sp, opposite[1 + i], source(w, (1 - zb) * 2 + (1 - x if i else x)), inner)
+
+    def along(w, k, only=None):
+        zb_, x_ = member_at(k)
+        start(w, index(za, zb_, y, x_), opposite[0], source(w, me) if k == 0 else None, only)
+
+    def gather(w, k):
+        with jax.named_scope(f"gather#w={w}#k={k}"):
+            zb_, x_ = member_at(k)
+            arrived(w, index(za, zb_, y, x_))
 
     def member_at(k):
         fz, fx = (0, 0) if k == 0 else flips[k - 1]
         return flip(zb, fz), flip(x, fx)
 
-    def spread(w, k):
-        with jax.named_scope(f"spread#w={w}#k={k}"):
-            zb_, x_ = member_at(k)
-            s = index(za, zb_, y, x_)
-            arrived(w, s)
-            along(w, s)
-
     def cross(w, k):
         zb_, x_ = member_at(k)
         start(w, index(za, zb_, y, x_), across, source(w, me) if k == 0 else None)
@@ -206,20 +213,18 @@
     def relay(w, k):
         with jax.named_scope(f"relay#w={w}#k={k}"):
             zb_, x_ = member_at(k)
-            for d in range(1, n_za):
-                s = index(lax.rem(za + n_za - d, n_za), zb_, y, x_)
-                arrived(w, s)
-                start(w, s, across)
-
-    def exchange(w):
-        for k in (1, 2, 0):
-            first_copy(w, k).start()
-        locals_[w].start()
-
-    exchange(0)
-    along(0, sp, source(0, me))
+            s = index(1 - za, zb_, y, x_)
+            arrived(w, s)
+            start(w, s, across)
+
+    for k in range(3):
+        first_copy(0, k).start()
+    locals_[0].start()
+    along(0, 0)
     cross(0, 0)
-    exchange(1)
+    direct(0, 0)
+    direct(0, 1)
+    locals_[1].start()
     load_wo = pltpu.make_async_copy(w_out, wo, loc_sem.at[0])
     load_wo.start()
     load_res = pltpu.make_async_copy(resid.at[pl.ds(t * half, half), :], res, loc_sem.at[1])
@@ -380,16 +385,25 @@
     for r in range(rounds):
         attend_block(r, 0)
         if r == 0:
-            spread(0, 1)
+            gather(0, 1)
+            along(0, 1)
             cross(0, 1)
+            for k in range(3):
+                first_copy(1, k).start()
+        if r == 1:
+            relay(0, 0)
+            relay(0, 1)
         attend_block(r, 1)
         if r == 0:
             for k in (2, 3):
-                spread(0, k)
+                gather(0, k)
+                along(0, k, inner)
                 cross(0, k)
             load_wo.wait()
             load_res.wait()
         one_round(r)
+        if r == 0:
+            direct(1, 0)
 
     def up(m):
         row = pl.multiple_of(m * rows, rows)
@@ -416,15 +430,29 @@
                 for k in range(4):
                     arrived(0, index(a, k // 2, 1 - y, k % 2))
 
-    along(1, sp, source(1, me))
-    for k in (1, 2, 3):
-        spread(1, k)
-    for k in range(4):
-        relay(0, k)
-    for k in range(4):
+    outer = jnp.logical_not(inner)
+    gather(1, 1)
+    for k in (0, 1):
+        along(1, k, outer)
+    if rounds < 2:
+        relay(0, 0)
+        relay(0, 1)
+    relay(0, 2)
+    relay(0, 3)
+    for k in (0, 1):
         cross(1, k)
-    for r in range(rounds):
+    token_pass(1, 0)
+    for k in (2, 3):
+        gather(1, k)
+        cross(1, k)
+    for r in range(1, rounds):
         token_pass(1, r)
+    direct(1, 1)
+
+    @pl.when(outer)
+    def _():
+        pl.semaphore_signal(credit, inc=1, device_id=opposite[0], device_id_type=MESH)
+
     finish_up()
     pair_wait(3)
     up(me)
@@ -432,13 +460,22 @@
         token_pass(0, r)
     pair_wait(0)
     up(member(0))
+    with jax.named_scope("credit_wait"):
+        @pl.when(inner)
+        def _():
+            pl.semaphore_wait(credit, 1)
+
+    for k in range(4):
+        along(1, k, inner)
     for r in range(rounds):
         token_pass(2, r)
-    relay(1, 0)
-    relay(1, 1)
+        if r == 0:
+            relay(1, 0)
     for k in (1, 2):
         pair_wait(k)
         up(member(k))
+        if k == 1:
+            relay(1, 1)
     locals_[1].wait()
 
     order = [(d, fz, fy) for d in range(n_za) for fy in range(2) for fz in range(2)]
@@ -549,17 +586,22 @@
             c.start()
 
     count = len(order)
-    for p in range(count + 3):
-        if p < count:
-            if p == 2:
-                relay(1, 2)
-            if p == 3:
-                relay(1, 3)
-            down(p)
-        if 1 <= p <= count:
+    early = count // 2
+    for p in range(early):
+        down(p)
+        if p:
             combine(p - 1)
-        if 3 <= p:
-            merge(p - 3)
+        if p == 0:
+            relay(1, 2)
+        if p == 2:
+            relay(1, 3)
+    for p in range(early, count):
+        down(p)
+        combine(p - 1)
+        merge(p - early)
+    combine(count - 1)
+    for p in range(early, count):
+        merge(p)
     for p in range(count):
         last(p)
     with jax.named_scope("final_wait"):
@@ -584,8 +626,11 @@
     for w in range(2):
         for k in range(3):
             first_copy(w, k).wait_send()
-        for c in sent[w]:
-            c.wait_send()
+        for c, only in sent[w]:
+            if only is None:
+                c.wait_send()
+            else:
+                pl.when(only)(c.wait_send)
     for r in range(rounds):
         for k in range(2):
             token_copy(k, r).wait_send()
@@ -703,7 +748,7 @@
     vmem = pl.BlockSpec(memory_space=pltpu.VMEM)
     smem = pl.BlockSpec(memory_space=pltpu.SMEM)
     hbm = pl.BlockSpec(memory_space=pl.ANY)
-    sends = 3 + 4 * n_za + 4 * (n_za - 1)
+    sends = 20
     block = 2 * w_down.shape[1]
     blocks = width // block
     dma = pltpu.SemaphoreType.DMA
@@ -757,6 +802,7 @@
             dma((blocks,)),
             dma((blocks,)),
             dma((blocks,)),
+            pltpu.SemaphoreType.REGULAR,
         ],
         compiler_params=pltpu.CompilerParams(
             collective_id=0, has_side_effects=True, vmem_limit_bytes=63 * 1024 * 1024
@@ -797,7 +843,7 @@
 
     def shards(*args):
         columns = args[11].shape[1]
-        fits = sizes["tp"] == 2 and sizes["sp"] % 8 == 0 and columns % 128 == 0
+        fits = sizes["tp"] == 2 and sizes["sp"] // 8 == 2 and sizes["sp"] % 8 == 0 and columns % 128 == 0
         return (fused_shards if fits else plain_shards)(*args)
 
     return jax.shard_map(

time: 173 us -> 160 us (0.925); the launches traced: 171 us -> 160 us
  Pallas kernels: 168 us -> 157 us
    pallas_call x1, Pallas kernels: 168 us -> 157 us  [fused_shards(): pl.pallas_call(functools.partial(kernel, n_sp, head, heads, kv_heads, slo...]
where the time goes in v2:
time: 160 us
  Pallas kernels  157 us (98%)
  local copies, waits for them, and re-layouts  3.16 us (2%)
    pallas_call x1, Pallas kernels, fused_shards(): pl.pallas_call(functools.partial(kernel, n_sp, head, heads, kv_heads, slo...  157 us

profile of v2, /device:TPU:13, one launch (start us, length us, event | category | flops | bytes accessed | tf_op | source)
XLA Modules:
  0.0 159.9 jit_solution(13569736341082107058)
XLA Ops:
  0.0 156.7 %layer.1 = bf16[512,2048]{1,0:T(8,128)(2,1)} custom-call(bf16[512,2048]{1,0:T(8,128)(2,1)} %resid.1, bf16[512,1024]{1,0:T(8,128)(2,1)} %queries.1, bf16[512,256]{1,0:T(8,128)(2,1)} %keys.1, bf16[512,256]{1,0:T(8,128)(2,1)} %values.1, s32[1,512]{1,0:T(1,128)} %bitcast.5, f32[1,64]{1,0:T(1,128)} %bitcast.6, f32[1,64]{1,0:T(1,128)} %bitcast.7, f32[16]{0:T(128)} %sink.1, ...), custom_call_target="tpu_custom_call" | custom-call | tf_op jit(solution)/shard_map/layer/pallas_call | solution.py:755
  156.7 3.2 %copy.14 = bf16[512,2048]{1,0:T(8,128)(2,1)} copy(bf16[512,2048]{1,0:T(8,128)(2,1)} %layer.1) | data formatting | bytes 4194304

commit v3 on v2

--- a/solution.py
+++ b/solution.py
@@ -88,7 +88,7 @@
     half = rows // 2
     depth = w_up.shape[0]
     units = wu.shape[1]
-    width = wd.shape[1]
+    width = resid.shape[1]
     group = heads // kv_heads
     n_za = n_sp // 8
     block = 2 * w_down.shape[1]
@@ -163,7 +163,7 @@
     def place(w, s):
         if w == 0:
             return wu.at[pl.ds(pl.multiple_of(s * depth, depth), depth), :]
-        return wd.at[:, pl.ds(pl.multiple_of(s * (block // 2), block // 2), block // 2)]
+        return wd.at[s]
 
     def source(w, m):
         at = pl.ds(pl.multiple_of(m * units, units), units)
@@ -467,19 +467,7 @@
 
     for k in range(4):
         along(1, k, inner)
-    for r in range(rounds):
-        token_pass(2, r)
-        if r == 0:
-            relay(1, 0)
-    for k in (1, 2):
-        pair_wait(k)
-        up(member(k))
-        if k == 1:
-            relay(1, 1)
-    locals_[1].wait()
-
     order = [(d, fz, fy) for d in range(n_za) for fy in range(2) for fz in range(2)]
-    chunks = 4
     ways = ((0, 1), (1, 0))
 
     def block_of(p):
@@ -487,71 +475,92 @@
         return lax.rem(za + n_za - d, n_za) * 4 + flip(zb, fz) * 2 + flip(y, fy)
 
     def axes(p):
-        return ways[0] if order[p][0] % 2 == 0 else ways[1]
+        return ways[1] if p >= len(order) - 2 else ways[0]
 
     def cols_of(g):
         return pl.ds(pl.multiple_of(g * block, block), block)
 
-    def twin_copy(g):
-        return remote(twin_out.at[g], twin_in.at[g], twin_send.at[g], twin_recv.at[g], (sp, u))
-
-    def first_sum(p):
+    def twin_copy(p, z):
+        at = (block_of(p), pl.ds(2 * z, 2))
+        return remote(twin_out.at[at], twin_in.at[at], twin_send.at[z, block_of(p)],
+                      twin_recv.at[z, block_of(p)], (sp, u))
+
+    def first_sum(p, i):
         g = block_of(p)
-        return remote(first_out.at[g], first_in.at[g], sum_send.at[0, g], sum_recv.at[0, g], near[axes(p)[0]])
+        return remote(first_out.at[g, i], first_in.at[g, i], sum_send.at[i, g], sum_recv.at[i, g],
+                      near[axes(p)[0]])
 
     def second_sum(p):
         g = block_of(p)
-        return remote(second_out.at[g], second_in.at[g], sum_send.at[1, g], sum_recv.at[1, g], near[axes(p)[1]])
-
-    def down(p):
-        d, fz, fy = order[p]
+        return remote(second_out.at[g], second_in.at[g], sum_send.at[2, g], sum_recv.at[2, g], near[axes(p)[1]])
+
+    pending = []
+    passes = [0]
+
+    def down(p, z):
         g = block_of(p)
-        with jax.named_scope(f"down_wait#p={p}"):
-            if fy == 1:
+        slot = passes[0] % 3
+        passes[0] += 1
+        if z == 0 and order[p][2] == 1:
+            with jax.named_scope(f"down_wait#p={p}"):
                 for i in range(2):
                     arrived(1, g * 2 + i)
-        cols = cols_of(g)
+        zb_ = flip(zb, z)
 
         def step(c, carry):
-            cz, cx = c // 2, c % 2
-            row = (zb + cz - 2 * zb * cz) * 2 + (x + cx - 2 * x * cx)
+            row = zb_ * 2 + (x + c - 2 * x * c)
             theirs = pl.ds(pl.multiple_of(row * rows + u * half, half), half)
             ours = pl.ds(pl.multiple_of(row * rows + t * half, half), half)
-            twin_out[g, c, :, :] = jnp.dot(act[theirs, :], wd[:, cols], preferred_element_type=F32).astype(BF16)
-            part[p % 2, c, :, :] = jnp.dot(act[ours, :], wd[:, cols], preferred_element_type=F32)
+            cols = jnp.concatenate([wd[g * 2], wd[g * 2 + 1]], axis=1)
+            twin_out[g, 2 * z + c, :, :] = jnp.dot(act[theirs, :], cols, preferred_element_type=F32).astype(BF16)
+            part[slot, c, :, :] = jnp.dot(act[ours, :], cols, preferred_element_type=F32)
             return carry
 
         with jax.named_scope("down"):
-            lax.fori_loop(0, chunks, step, 0)
-        twin_copy(g).start()
-
-    def combine(p):
+            lax.fori_loop(0, 2, step, 0)
+        twin_copy(p, z).start()
+        pending.append((p, z, slot))
+        if len(pending) > 2:
+            combine(*pending.pop(0))
+
+    def flush():
+        while pending:
+            combine(*pending.pop(0))
+
+    def combine(p, z, slot):
         g = block_of(p)
         cols = cols_of(g)
-        one, two = axes(p)
+        x_first = axes(p)[0] == 0
         with jax.named_scope("twin_wait"):
-            twin_copy(g).wait_recv()
+            twin_copy(p, z).wait_recv()
 
         def add(i, carry):
             at = pl.ds(pl.multiple_of(i * 64, 64), 64)
 
             def whole(c):
-                return part[p % 2, c, at, :] + twin_in[g, c, at, :].astype(F32)
-
-            first_out[g, 0, at, :] = whole(3).astype(BF16)
-            first_out[g, 1, at, :] = whole(one + 1).astype(BF16)
-            waiting[g, at, :] = whole(two + 1)
-            total[g, at, :] = whole(0) + mid[at, cols].astype(F32)
+                return part[slot, c, at, :] + twin_in[g, 2 * z + c, at, :].astype(F32)
+
+            if z == 0:
+                total[g, at, :] = whole(0) + mid[at, cols].astype(F32)
+            else:
+                first_out[g, 0, at, :] = whole(1).astype(BF16)
+            if x_first == (z == 0):
+                first_out[g, 1, at, :] = whole(1 - z).astype(BF16)
+            else:
+                waiting[g, at, :] = whole(1 - z)
             return carry
 
         with jax.named_scope("combine"):
             lax.fori_loop(0, half // 64, add, 0)
-        first_sum(p).start()
+        if z == 1:
+            first_sum(p, 0).start()
+        if x_first == (z == 0):
+            first_sum(p, 1).start()
 
     def merge(p):
         g = block_of(p)
         with jax.named_scope(f"merge_wait#p={p}"):
-            first_sum(p).wait_recv()
+            first_sum(p, 0).wait_recv()
 
         def add(i, carry):
             at = pl.ds(pl.multiple_of(i * 64, 64), 64)
@@ -573,6 +582,7 @@
     def last(p):
         g = block_of(p)
         with jax.named_scope(f"sum_wait#p={p}"):
+            first_sum(p, 1).wait_recv()
             second_sum(p).wait_recv()
 
         def add(i, carry):
@@ -587,19 +597,31 @@
 
     count = len(order)
     early = count // 2
+    locals_[1].wait()
+    down(0, 0)
+    down(1, 0)
+    token_pass(2, 0)
+    down(2, 0)
+    down(3, 0)
+    flush()
+    relay(1, 0)
+    for r in range(1, rounds):
+        token_pass(2, r)
+    pair_wait(1)
+    up(member(1))
+    relay(1, 1)
+    pair_wait(2)
+    up(member(2))
+    relay(1, 2)
     for p in range(early):
-        down(p)
-        if p:
-            combine(p - 1)
-        if p == 0:
-            relay(1, 2)
-        if p == 2:
+        down(p, 1)
+        if p == 1:
             relay(1, 3)
     for p in range(early, count):
-        down(p)
-        combine(p - 1)
+        down(p, 0)
+        down(p, 1)
         merge(p - early)
-    combine(count - 1)
+    flush()
     for p in range(early, count):
         merge(p)
     for p in range(count):
@@ -638,8 +660,9 @@
         for k in range(4):
             pair_copy(k, t, r).wait_send()
     for p in range(count):
-        twin_copy(block_of(p)).wait_send()
-        first_sum(p).wait_send()
+        for i in range(2):
+            twin_copy(p, i).wait_send()
+            first_sum(p, i).wait_send()
         second_sum(p).wait_send()
 
 
@@ -771,9 +794,9 @@
             pltpu.VMEM((half, width), BF16),
             pltpu.VMEM((MEMBERS * rows, width), BF16),
             pltpu.VMEM((width, units), BF16),
-            pltpu.VMEM((units, width), BF16),
+            pltpu.VMEM((n_sp, units, w_down.shape[1]), BF16),
             pltpu.VMEM((MEMBERS * rows, units), BF16),
-            pltpu.VMEM((2, MEMBERS, half, block), F32),
+            pltpu.VMEM((3, 2, half, block), F32),
             pltpu.VMEM((blocks, MEMBERS, half, block), BF16),
             pltpu.VMEM((blocks, MEMBERS, half, block), BF16),
             pltpu.VMEM((blocks, 2, half, block), BF16),
@@ -795,10 +818,10 @@
             dma((4, rounds)),
             dma((rounds,)),
             dma((rounds,)),
-            dma((blocks,)),
-            dma((blocks,)),
             dma((2, blocks)),
             dma((2, blocks)),
+            dma((3, blocks)),
+            dma((3, blocks)),
             dma((blocks,)),
             dma((blocks,)),
             dma((blocks,)),

time: 160 us -> 150 us (0.938)
  Pallas kernels: 157 us -> 147 us
    pallas_call x1, Pallas kernels: 157 us -> 147 us  [fused_shards(): pl.pallas_call(functools.partial(kernel, n_sp, head, heads, kv_heads, slo...]
where the time goes in v3:
time: 150 us
  Pallas kernels  147 us (98%)
  local copies, waits for them, and re-layouts  3.16 us (2%)
    pallas_call x1, Pallas kernels, fused_shards(): pl.pallas_call(functools.partial(kernel, n_sp, head, heads, kv_heads, slo...  147 us
    unnamed x1, local copies, waits for them, and re-layouts  3.16 us

profile of v3, /device:TPU:13, one launch (start us, length us, event | category | flops | bytes accessed | tf_op | source)
XLA Modules:
  0.0 149.7 jit_solution(4539934247960356552)
XLA Ops:
  0.0 146.5 %layer.1 = bf16[512,2048]{1,0:T(8,128)(2,1)} custom-call(bf16[512,2048]{1,0:T(8,128)(2,1)} %resid.1, bf16[512,1024]{1,0:T(8,128)(2,1)} %queries.1, bf16[512,256]{1,0:T(8,128)(2,1)} %keys.1, bf16[512,256]{1,0:T(8,128)(2,1)} %values.1, s32[1,512]{1,0:T(1,128)} %bitcast.5, f32[1,64]{1,0:T(1,128)} %bitcast.6, f32[1,64]{1,0:T(1,128)} %bitcast.7, f32[16]{0:T(128)} %sink.1, ...), custom_call_target="tpu_custom_call" | custom-call | tf_op jit(solution)/shard_map/layer/pallas_call | solution.py:778
  146.5 3.2 %copy.14 = bf16[512,2048]{1,0:T(8,128)(2,1)} copy(bf16[512,2048]{1,0:T(8,128)(2,1)} %layer.1) | data formatting | bytes 4194304

commit v4 on v3

--- a/solution.py
+++ b/solution.py
@@ -475,7 +475,7 @@
         return lax.rem(za + n_za - d, n_za) * 4 + flip(zb, fz) * 2 + flip(y, fy)
 
     def axes(p):
-        return ways[1] if p >= len(order) - 2 else ways[0]
+        return ways[1] if order[p][0] == 1 and order[p][2] == 0 else ways[0]
 
     def cols_of(g):
         return pl.ds(pl.multiple_of(g * block, block), block)
@@ -609,20 +609,23 @@
         token_pass(2, r)
     pair_wait(1)
     up(member(1))
-    relay(1, 1)
     pair_wait(2)
     up(member(2))
+    relay(1, 1)
+    for p in range(early - 1):
+        down(p, 1)
+    flush()
     relay(1, 2)
-    for p in range(early):
-        down(p, 1)
-        if p == 1:
-            relay(1, 3)
+    down(early - 1, 1)
+    flush()
+    relay(1, 3)
     for p in range(early, count):
         down(p, 0)
         down(p, 1)
         merge(p - early)
     flush()
-    for p in range(early, count):
+    late = tuple(range(early + 2, count))
+    for p in late[:1] + (early,) + late[1:] + (early + 1,):
         merge(p)
     for p in range(count):
         last(p)

time: 150 us -> 146 us (0.973)
  Pallas kernels: 147 us -> 141 us
    pallas_call x1, Pallas kernels: 147 us -> 141 us  [fused_shards(): pl.pallas_call(functools.partial(kernel, n_sp, head, heads, kv_heads, slo...]
where the time goes in v4:
time: 146 us; the launch traced here: 144 us
  Pallas kernels  141 us (97%)
  local copies, waits for them, and re-layouts  3.16 us (2%)
    pallas_call x1, Pallas kernels, fused_shards(): pl.pallas_call(functools.partial(kernel, n_sp, head, heads, kv_heads, slo...  141 us
    unnamed x1, local copies, waits for them, and re-layouts  3.16 us

profile of v4, /device:TPU:13, one launch (start us, length us, event | category | flops | bytes accessed | tf_op | source)
XLA Modules:
  0.0 144.2 jit_solution(11755110698625617949)
XLA Ops:
  0.0 141.0 %layer.1 = bf16[512,2048]{1,0:T(8,128)(2,1)} custom-call(bf16[512,2048]{1,0:T(8,128)(2,1)} %resid.1, bf16[512,1024]{1,0:T(8,128)(2,1)} %queries.1, bf16[512,256]{1,0:T(8,128)(2,1)} %keys.1, bf16[512,256]{1,0:T(8,128)(2,1)} %values.1, s32[1,512]{1,0:T(1,128)} %bitcast.5, f32[1,64]{1,0:T(1,128)} %bitcast.6, f32[1,64]{1,0:T(1,128)} %bitcast.7, f32[16]{0:T(128)} %sink.1, ...), custom_call_target="tpu_custom_call" | custom-call | tf_op jit(solution)/shard_map/layer/pallas_call | solution.py:781
  141.0 3.2 %copy.14 = bf16[512,2048]{1,0:T(8,128)(2,1)} copy(bf16[512,2048]{1,0:T(8,128)(2,1)} %layer.1) | data formatting | bytes 4194304
